TPU v7x, 32 devices: a whole 2x2x4 slice. The times are simulated.
32 devices in a mesh: grp: 2 (over y), sp: 4 (over z), tp: 4 (over x, core).
Axes of the slice: x: 2, y: 2, z: 4, core: 2. Of those that a mesh axis runs over, the one named last changes fastest.
Arguments:
- queries: bfloat16 [8192, 1024], P(('grp', 'sp'), 'tp'), parts along dimension 0, may hold values from -6 to 6
- keys: bfloat16 [8192, 256], P(('grp', 'sp')), parts along dimension 0, may hold values from -6 to 6
- values: bfloat16 [8192, 256], P(('grp', 'sp')), parts along dimension 0, may hold values from -6 to 6
- query_gain: float32 [128], replicated, may hold values from 1.2 to 6, as said below
- key_gain: float32 [128], replicated, may hold values from 1.2 to 6, as said below
- out_weight: bfloat16 [1024, 2048], replicated, may hold values from -6 to 6
- residual_in: bfloat16 [8192, 2048], P(('grp', 'sp', 'tp')), parts along dimension 0, may hold values from -6 to 6
- norm_gain: float32 [2048], replicated, may hold values from 0.1 to 1.9
- gate_weight: bfloat16 [2048, 2816], P('sp', 'tp'), may hold values from -0.125 to 0.125
- up_weight: bfloat16 [2048, 2816], P('sp', 'tp'), may hold values from -0.125 to 0.125
- down_weight: bfloat16 [2816, 2048], P('tp', 'sp'), may hold values from -0.109375 to 0.109375
Outputs:
- layer_out: bfloat16 [8192, 2048], P(('grp', 'sp', 'tp')), parts along dimension 0
There are 2 independent parts, one for each index of `grp`. A program takes and returns all parts, laid end to end along the dimension named above; an argument that names none is the same for every part. Nothing has to cross between parts.
Inputs may be any that keep to these rules, and one draw needn't show every extreme that they name: `query_gain`: positive gains. `key_gain`: positive gains.
All inputs are finite; a program needn't handle non-finite values.
Results may differ from a plain program's by a relative error of at most 0.015.
The roundings to bfloat16 on the way count: a program that leaves them out, or rounds other values in their place, can miss the bound.
Values may be sent and summed in bfloat16 or wider, within the bound.
A program may use at most 128 MiB of HBM per device.

v0:
```python
import jax
import jax.numpy as jnp
from jax import lax
from jax.sharding import PartitionSpec as P

HQ = 8
KV = 2
HD = 128
GRID_W = 64


def rotate(widened, positions):
    half = HD // 2
    inverse = 10000.0 ** (-jnp.arange(0, half, 2, dtype=jnp.float32) / half)
    grid_row = (positions // GRID_W).astype(jnp.float32)
    grid_col = (positions % GRID_W).astype(jnp.float32)
    angles = jnp.concatenate(
        [grid_row[:, None] * inverse[None], grid_col[:, None] * inverse[None]], axis=-1
    )
    cosine = jnp.cos(angles)[:, None, :]
    sine = jnp.sin(angles)[:, None, :]
    pairs = widened.reshape(widened.shape[0], widened.shape[1], half, 2)
    first = pairs[..., 0]
    second = pairs[..., 1]
    turned = jnp.stack([first * cosine - second * sine, first * sine + second * cosine], axis=-1)
    return turned.reshape(widened.shape)


def prepare(source, gain, positions, heads):
    widened = source.astype(jnp.float32).reshape(source.shape[0], heads, HD)
    widened = (
        widened * lax.rsqrt(jnp.mean(widened * widened, axis=-1, keepdims=True) + 1e-06) * gain
    )
    return rotate(widened, positions).astype(jnp.bfloat16)


def local(
    queries,
    keys,
    values,
    query_gain,
    key_gain,
    out_weight,
    residual_in,
    norm_gain,
    gate_weight,
    up_weight,
    down_weight,
):
    tok_rows = queries.shape[0]
    heads_here = queries.shape[1] // HD
    seq_index = lax.axis_index("sp")
    head_index = lax.axis_index("tp")
    positions = seq_index * tok_rows + jnp.arange(tok_rows, dtype=jnp.int32)
    query_rot = prepare(queries, query_gain, positions, heads_here)
    query_rot = query_rot.transpose(1, 0, 2).reshape(heads_here * tok_rows, HD)
    pair_index = head_index * heads_here // (HQ // KV)
    key_block = lax.dynamic_slice_in_dim(keys, pair_index * HD, HD, 1)
    value_block = lax.dynamic_slice_in_dim(values, pair_index * HD, HD, 1)
    key_rot = prepare(key_block, key_gain, positions, 1).reshape(tok_rows, HD)
    scale = HD ** (-0.5)

    def attend_block(carry, block):
        running_max, denominator, weighted = carry
        key_part, value_part = block
        scores = (
            lax.dot_general(
                query_rot, key_part, (((1,), (1,)), ((), ())), preferred_element_type=jnp.float32
            )
            * scale
        )
        new_max = jnp.maximum(running_max, jnp.max(scores, axis=1))
        factor = jnp.exp(running_max - new_max)
        raised = jnp.exp(scores - new_max[:, None])
        denominator = denominator * factor + jnp.sum(raised, axis=1)
        weighted = weighted * factor[:, None] + jnp.dot(
            raised.astype(jnp.bfloat16), value_part, preferred_element_type=jnp.float32
        )
        return ((new_max, denominator, weighted), None)

    start_carry = (
        jnp.full((heads_here * tok_rows,), -1e30, jnp.float32),
        jnp.zeros((heads_here * tok_rows,), jnp.float32),
        jnp.zeros((heads_here * tok_rows, HD), jnp.float32),
    )
    carry = start_carry
    pieces = (
        lax.all_gather(key_rot, "sp", axis=0, tiled=True),
        lax.all_gather(value_block, "sp", axis=0, tiled=True),
    )
    length = pieces[0].shape[0]
    block = tok_rows
    count = length // block
    key_parts = pieces[0].reshape(count, block, HD)
    value_parts = pieces[1].reshape(count, block, HD)
    carry, unused = lax.scan(attend_block, carry, (key_parts, value_parts))
    running_max, denominator, weighted = carry
    attended = (weighted / denominator[:, None]).astype(jnp.bfloat16)
    attended = (
        attended.reshape(heads_here, tok_rows, HD)
        .transpose(1, 0, 2)
        .reshape(tok_rows, heads_here * HD)
    )
    traded = lax.all_to_all(attended, "tp", split_axis=0, concat_axis=1, tiled=True)
    projected = jnp.dot(traded, out_weight, preferred_element_type=jnp.float32)
    middle = residual_in.astype(jnp.float32) + projected
    normed = (
        middle * lax.rsqrt(jnp.mean(middle * middle, axis=-1, keepdims=True) + 1e-06) * norm_gain
    )
    normed = normed.astype(jnp.bfloat16)
    rows_all = lax.all_gather(normed, "tp", axis=0, tiled=True)
    pieces = (
        lax.all_gather(gate_weight, "sp", axis=0, tiled=True),
        lax.all_gather(up_weight, "sp", axis=0, tiled=True),
    )
    gate_act = jnp.dot(rows_all, pieces[0], preferred_element_type=jnp.float32)
    up_act = jnp.dot(rows_all, pieces[1], preferred_element_type=jnp.float32)
    down_all = lax.all_gather(down_weight, "sp", axis=1, tiled=True)
    hidden = (jax.nn.silu(gate_act) * up_act).astype(jnp.bfloat16)
    mixer_out = lax.psum_scatter(
        jnp.dot(hidden, down_all, preferred_element_type=jnp.float32).astype(jnp.bfloat16),
        "tp",
        scatter_dimension=0,
        tiled=True,
    ).astype(jnp.float32)
    return (middle + mixer_out).astype(jnp.bfloat16)


def solution(mesh):
    placed = (
        P(("grp", "sp"), "tp"),
        P(("grp", "sp"), None),
        P(("grp", "sp"), None),
        P(),
        P(),
        P(),
        P(("grp", "sp", "tp"), None),
        P(),
        P("sp", "tp"),
        P("sp", "tp"),
        P("tp", "sp"),
    )
    return jax.shard_map(
        local, mesh=mesh, in_specs=placed, out_specs=P(("grp", "sp", "tp"), None), check_vma=False
    )
```

profile of v0, /device:TPU:0, one launch (start us, length us, event | category | flops | bytes accessed | tf_op | source)
XLA Modules:
  0.0 361.1 jit_solution(3886411990185898844)
XLA Ops:
  6.6 1.2 fusion.18
  7.8 1.2 fusion.19
  9.0 0.2 copy.31
  9.2 0.3 reshape.338
  9.5 0.4 fusion.34
  9.9 0.1 broadcast_multiply_fusion.1
  10.1 1.0 subtract_convert_fusion.1
  11.2 0.3 copy.34
  11.4 0.8 convert_element_type.62
  12.3 0.0 all-gather.9.cloned.1.call-start
  12.3 0.7 constant_dynamic-slice_fusion
  13.1 0.0 all-gather.13.cloned.1.call-start
  13.1 0.7 all-gather.13.cloned.1.call-update
  13.9 1.0 convert_multiply_fusion.2
  14.9 0.2 copy.35
  15.2 2.7 mul.248
  17.9 2.4 reduce_sum.37
  20.3 0.2 copy.36
  20.5 1.6 reshape.340
  22.1 0.1 mul.251
  22.3 1.1 fusion.21
  23.4 1.7 multiply_multiply_fusion
  25.1 1.4 subtract_convert_fusion
  26.5 1.2 pad_maximum_fusion
  27.7 0.5 copy.37
  28.3 0.5 copy.43
  28.8 14.3 %all-gather.7.cloned.1.call-done = bf16[4096,128]{0,1:T(8,128)(2,1)} async-done(((bf16[1024,128]{0,1:T(8,128)(2,1)}), bf16[4096,128]{0,1:T(8,128)(2,1)}) %all-gather.7.cloned.1.call-update) | async-done | bytes 1048592 | tf_op jit(solution)/shard_map/all_gather | solution.py:88
  43.1 1.6 copy.42
  44.7 27.3 %all-gather.9.cloned.1.call-done = bf16[4096,128]{1,0:T(8,128)(2,1)} async-done(((bf16[1024,128]{1,0:T(8,128)(2,1)}), bf16[4096,128]{1,0:T(8,128)(2,1)}) %all-gather.9.cloned.1.call-update) | async-done | bytes 1048592 | tf_op jit(solution)/shard_map/all_gather | solution.py:89
  72.1 53.6 %while.15 = (s32[]{:T(128)}, f32[2048]{0:T(1024)S(1)}, f32[2048]{0:T(1024)S(1)}, f32[2048,128]{1,0:T(8,128)S(1)}, bf16[4,1024,128]{2,1,0:T(8,128)(2,1)S(1)}, /*i...) while((s32[]{:T(128)}, f32[2048]{0:T(1024)S(1)}, ...), condition=%wide.region_5.6_spmd.clone, body=%wide.region_2.5_spmd.clone.sunk | while | flops 1091315712 | bytes 61997704 | solution.py:96
  72.1 4.5 %multiply_reduce_fusion.3 = (f32[2048]{0:T(1024)S(1)}, f32[1024,2048]{1,0:T(8,128)}) fusion(bf16[2048,128]{1,0:T(8,128)(2,1)S(1)} %get-tuple-element.200, bf16[4,1024,128]{2,1,0:T(8,128)(2,1)S(1)} %get-tuple-element.199, s32[]{:T(128)} %get-tuple-element.186), kind=kOutput, calls=%fused_computation.1.clone.1 | convolution fusion | flops 541063168 | bytes 9183236 | tf_op jit(solution)/shard_map/while/body/eval_jaxpr/dot_general | solution.py:67
  76.6 5.1 %fusion.53 = f32[2048]{0:T(1024)S(1)} fusion(f32[1024,2048]{1,0:T(8,128)} %get-tuple-element.174, f32[2048]{0:T(1024)S(1)} %select_maximum_fusion.2), kind=kLoop, calls=%fused_computation.3.clone.1 | loop fusion | flops 6289408 | bytes 8404992 | tf_op jit(solution)/shard_map/while/body/eval_jaxpr/reduce_sum | solution.py:75
  81.7 1.3 copy-done.1
  83.0 2.9 fusion.55
  86.0 4.5 %multiply_reduce_fusion.3 = (f32[2048]{0:T(1024)S(1)}, f32[1024,2048]{1,0:T(8,128)}) fusion(bf16[2048,128]{1,0:T(8,128)(2,1)S(1)} %get-tuple-element.200, bf16[4,1024,128]{2,1,0:T(8,128)(2,1)S(1)} %get-tuple-element.199, s32[]{:T(128)} %get-tuple-element.186), kind=kOutput, calls=%fused_computation.1.clone.1 | convolution fusion | flops 541063168 | bytes 9183236 | tf_op jit(solution)/shard_map/while/body/eval_jaxpr/dot_general | solution.py:67
  90.5 5.0 %fusion.53 = f32[2048]{0:T(1024)S(1)} fusion(f32[1024,2048]{1,0:T(8,128)} %get-tuple-element.174, f32[2048]{0:T(1024)S(1)} %select_maximum_fusion.2), kind=kLoop, calls=%fused_computation.3.clone.1 | loop fusion | flops 6289408 | bytes 8404992 | tf_op jit(solution)/shard_map/while/body/eval_jaxpr/reduce_sum | solution.py:75
  95.4 0.9 copy-done.1
  96.3 2.9 fusion.55
  99.2 4.5 %multiply_reduce_fusion.3 = (f32[2048]{0:T(1024)S(1)}, f32[1024,2048]{1,0:T(8,128)}) fusion(bf16[2048,128]{1,0:T(8,128)(2,1)S(1)} %get-tuple-element.200, bf16[4,1024,128]{2,1,0:T(8,128)(2,1)S(1)} %get-tuple-element.199, s32[]{:T(128)} %get-tuple-element.186), kind=kOutput, calls=%fused_computation.1.clone.1 | convolution fusion | flops 541063168 | bytes 9183236 | tf_op jit(solution)/shard_map/while/body/eval_jaxpr/dot_general | solution.py:67
  103.7 5.0 %fusion.53 = f32[2048]{0:T(1024)S(1)} fusion(f32[1024,2048]{1,0:T(8,128)} %get-tuple-element.174, f32[2048]{0:T(1024)S(1)} %select_maximum_fusion.2), kind=kLoop, calls=%fused_computation.3.clone.1 | loop fusion | flops 6289408 | bytes 8404992 | tf_op jit(solution)/shard_map/while/body/eval_jaxpr/reduce_sum | solution.py:75
  108.7 0.8 copy-done.1
  109.6 2.9 fusion.55
  112.5 4.5 %multiply_reduce_fusion.3 = (f32[2048]{0:T(1024)S(1)}, f32[1024,2048]{1,0:T(8,128)}) fusion(bf16[2048,128]{1,0:T(8,128)(2,1)S(1)} %get-tuple-element.200, bf16[4,1024,128]{2,1,0:T(8,128)(2,1)S(1)} %get-tuple-element.199, s32[]{:T(128)} %get-tuple-element.186), kind=kOutput, calls=%fused_computation.1.clone.1 | convolution fusion | flops 541063168 | bytes 9183236 | tf_op jit(solution)/shard_map/while/body/eval_jaxpr/dot_general | solution.py:67
  117.0 5.0 %fusion.53 = f32[2048]{0:T(1024)S(1)} fusion(f32[1024,2048]{1,0:T(8,128)} %get-tuple-element.174, f32[2048]{0:T(1024)S(1)} %select_maximum_fusion.2), kind=kLoop, calls=%fused_computation.3.clone.1 | loop fusion | flops 6289408 | bytes 8404992 | tf_op jit(solution)/shard_map/while/body/eval_jaxpr/reduce_sum | solution.py:75
  122.0 0.8 copy-done.1
  122.8 2.9 fusion.55
  125.7 0.3 divide_convert_fusion
  126.1 0.5 copy.51
  126.6 0.3 all_to_all.14
  126.9 11.2 %all_to_all.19 = bf16[4,256,256]{2,1,0:T(8,128)(2,1)S(1)} all-to-all(bf16[4,256,256]{2,1,0:T(8,128)(2,1)S(1)} %all_to_all.14), channel_id=1, replica_groups=mesh['grp'=2,'sp'=4,'tp'=4] {'tp'}, dimensions={0} | all-to-all | bytes 1048576 | tf_op jit(solution)/shard_map/all_to_all | solution.py:104
  138.2 0.2 copy.41
  138.4 3.9 %multiply_reduce_fusion.1 = (f32[256]{0:T(256)S(1)}, f32[256,2048]{1,0:T(8,128)S(1)}) fusion(bf16[256,1024]{0,1:T(8,128)(2,1)S(1)} %bitcast.46, bf16[1024,2048]{1,0:T(8,128)(2,1)} %param.18, bf16[256,2048]{1,0:T(8,128)(2,1)} %param.19), kind=kOutput, calls=%fused_computation.26 | convolution fusion | flops 1075838720 | bytes 7865344 | tf_op jit(solution)/shard_map/dot_general | solution.py:105
  142.3 1.2 multiply_convert_fusion.1
  143.5 0.0 all-gather.15.cloned.1.call-start
  143.6 0.5 all-gather.15.cloned.1.call-update
  144.2 0.5 all-gather.17.cloned.1.call-update
  144.7 0.3 reduce-scatter.2.cloned.1.call-start
  145.0 31.5 %all-gather.11.cloned.1.call-done = bf16[1024,2048]{1,0:T(8,128)(2,1)} async-done(((bf16[256,2048]{1,0:T(8,128)(2,1)}), bf16[1024,2048]{1,0:T(8,128)(2,1)}) %all-gather.11.cloned.1.call-update) | async-done | bytes 4194320 | tf_op jit(solution)/shard_map/all_gather | solution.py:111
  176.5 7.8 %fusion.35 = f32[1024,704]{0,1:T(8,128)} fusion(bf16[1024,2048]{1,0:T(8,128)(2,1)} %all-gather.11.cloned.1.call-done, bf16[2048,704]{0,1:T(8,128)(2,1)} %all-gather.13.cloned.1.call-done), kind=kOutput, calls=%fused_computation.72 | convolution fusion | flops 2952790016 | bytes 9961472 | tf_op jit(solution)/shard_map/dot_general | solution.py:116
  184.3 52.7 %all-gather.15.cloned.1.call-done = bf16[2048,704]{0,1:T(8,128)(2,1)} async-done(((bf16[512,704]{0,1:T(8,128)(2,1)}), bf16[2048,704]{0,1:T(8,128)(2,1)}) %all-gather.15.cloned.1.call-update) | async-done | bytes 2883600 | tf_op jit(solution)/shard_map/all_gather | solution.py:114
  237.1 59.3 %all-gather.17.cloned.1.call-done = bf16[704,2048]{1,0:T(8,128)(2,1)} async-done(((bf16[704,512]{1,0:T(8,128)(2,1)}), bf16[704,2048]{1,0:T(8,128)(2,1)}) %all-gather.17.cloned.1.call-update) | async-done | bytes 2883600 | tf_op jit(solution)/shard_map/all_gather | solution.py:118
  296.3 12.0 %convolution_convert_fusion = bf16[1024,2048]{1,0:T(8,128)(2,1)} fusion(bf16[704,2048]{1,0:T(8,128)(2,1)} %all-gather.17.cloned.1.call-done, f32[1024,704]{0,1:T(8,128)} %fusion.35, bf16[1024,2048]{1,0:T(8,128)(2,1)} %all-gather.11.cloned.1.call-done, bf16[2048,704]{0,1:T(8,128)(2,1)} %all-gather.15.cloned.1.call-done), kind=kOutput, calls=%fused_computation.21 | convolution fusion | flops 5912002560 | bytes 17039360 | tf_op jit(solution)/shard_map/dot_general | solution.py:121
  308.4 43.4 %reduce-scatter.2.cloned.1.call-done = bf16[256,2048]{1,0:T(8,128)(2,1)} async-done(((bf16[1024,2048]{1,0:T(8,128)(2,1)}), bf16[256,2048]{1,0:T(8,128)(2,1)}) %reduce-scatter.2.cloned.1.call-update) | async-done | bytes 1048592 | tf_op jit(solution)/shard_map/reduce_scatter | solution.py:120
  351.8 2.5 add_convert_fusion
  (41 shorter events, 0.4 us)
Async XLA Ops:
  6.5 5.8 %copy-start = (bf16[1024,256]{1,0:T(8,128)(2,1)S(1)}, bf16[1024,256]{1,0:T(8,128)(2,1)}, u32[]{:S(2)}) copy-start(bf16[1024,256]{1,0:T(8,128)(2,1)} %param.15) | copy-start | bytes 1572868
  6.5 36.6 %all-gather.7.cloned.1.call-start = ((), (), s32[]{:S(2)}) async-start(), calls=%async_computation.2 | async-start | bytes 1310720 | tf_op jit(solution)/shard_map/all_gather | solution.py:88
  9.5 4.4 %copy-start.2 = (bf16[1024,256]{1,0:T(8,128)(2,1)S(1)}, bf16[1024,256]{1,0:T(8,128)(2,1)}, u32[]{:S(2)}) copy-start(bf16[1024,256]{1,0:T(8,128)(2,1)} %param.13) | copy-start | bytes 1572868
  12.3 59.8 %all-gather.9.cloned.1.call-start = ((), (), s32[]{:S(2)}) async-start(), calls=%async_computation.3 | async-start | bytes 1310720 | tf_op jit(solution)/shard_map/all_gather | solution.py:89
  13.1 131.9 %all-gather.13.cloned.1.call-start = ((), (), s32[]{:S(2)}) async-start(), calls=%async_computation.5 | async-start | bytes 3604480 | tf_op jit(solution)/shard_map/all_gather | solution.py:113
  13.8 162.7 %all-gather.11.cloned.1.call-start = ((), (), s32[]{:S(2)}) async-start(), calls=%async_computation.4 | async-start | bytes 5242880 | tf_op jit(solution)/shard_map/all_gather | solution.py:111
  15.2 7.0 %copy-start.4 = (f32[128]{0:T(128)S(1)}, f32[128]{0:T(128)}, u32[]{:S(2)}) copy-start(f32[128]{0:T(128)} %param.16) | copy-start | bytes 1540
  76.6 6.5 %copy-start.1 = (f32[1024,2048]{1,0:T(8,128)S(1)}, f32[1024,2048]{1,0:T(8,128)}, u32[]{:S(2)}) copy-start(f32[1024,2048]{1,0:T(8,128)} %get-tuple-element.174) | copy-start | bytes 25165828 | tf_op jit(solution)/shard_map/while
  90.5 5.9 %copy-start.1 = (f32[1024,2048]{1,0:T(8,128)S(1)}, f32[1024,2048]{1,0:T(8,128)}, u32[]{:S(2)}) copy-start(f32[1024,2048]{1,0:T(8,128)} %get-tuple-element.174) | copy-start | bytes 25165828 | tf_op jit(solution)/shard_map/while
  103.7 5.8 %copy-start.1 = (f32[1024,2048]{1,0:T(8,128)S(1)}, f32[1024,2048]{1,0:T(8,128)}, u32[]{:S(2)}) copy-start(f32[1024,2048]{1,0:T(8,128)} %get-tuple-element.174) | copy-start | bytes 25165828 | tf_op jit(solution)/shard_map/while
  117.0 5.8 %copy-start.1 = (f32[1024,2048]{1,0:T(8,128)S(1)}, f32[1024,2048]{1,0:T(8,128)}, u32[]{:S(2)}) copy-start(f32[1024,2048]{1,0:T(8,128)} %get-tuple-element.174) | copy-start | bytes 25165828 | tf_op jit(solution)/shard_map/while
  138.4 3.9 %copy-start.3 = (f32[2048]{0:T(1024)S(1)}, f32[2048]{0:T(1024)}, u32[]{:S(2)}) copy-start(f32[2048]{0:T(1024)} %param.20) | copy-start | bytes 24580
  143.5 93.5 %all-gather.15.cloned.1.call-start = ((), (), s32[]{:S(2)}) async-start(), calls=%async_computation.6 | async-start | bytes 3604480 | tf_op jit(solution)/shard_map/all_gather | solution.py:114
  144.1 152.2 %all-gather.17.cloned.1.call-start = ((), (), s32[]{:S(2)}) async-start(), calls=%async_computation.7 | async-start | bytes 3604480 | tf_op jit(solution)/shard_map/all_gather | solution.py:118
  144.7 207.1 %reduce-scatter.2.cloned.1.call-start = ((), (), s32[]{:S(2)}) async-start(), calls=%async_computation.8 | async-start | bytes 5242880 | tf_op jit(solution)/shard_map/reduce_scatter | solution.py:120
Sparse Core Ops, SparseCore 0:
  12.4 30.6 all-gather.6
  44.7 27.3 all-gather.8
  73.7 58.4 all-gather.12
  143.6 32.8 all-gather.10
  177.9 59.1 all-gather.14
  238.5 57.7 all-gather.16
  308.5 43.2 reduce-scatter.1
where the time goes:
time: 362 us; the launch traced here: 361 us
  waiting for transfers between devices  230 us (64%)
  matrix products  53.2 us (15%)
  other arithmetic  36.6 us (10%)
  local copies, waits for them, and re-layouts  15.3 us (4%)
  between operations  13.8 us (4%)
  blocking collectives  11.2 us (3%)
    all_gather x1, waiting for transfers between devices, local(): down_all = lax.all_gather(down_weight, 'sp', axis=1, tiled=True)  59.3 us
    all_gather x1, waiting for transfers between devices, local(): lax.all_gather(up_weight, 'sp', axis=0, tiled=True)  52.7 us
    reduce_scatter x1, waiting for transfers between devices, local(): lax.psum_scatter(jnp.dot(hidden, down_all, preferred_element_type=jnp.flo...  43.4 us
    all_gather x1, waiting for transfers between devices, local(): rows_all = lax.all_gather(normed, 'tp', axis=0, tiled=True)  31.5 us
    all_gather x1, waiting for transfers between devices, local(): lax.all_gather(value_block, 'sp', axis=0, tiled=True)  27.3 us
    reduce_sum x4, other arithmetic, attend_block(): denominator = denominator * factor + jnp.sum(raised, axis=1)  20 us
    dot_general x4, matrix products, attend_block(): lax.dot_general(query_rot, key_part, (((1,), (1,)), ((), ())), preferred_...  18 us
    all_gather x1, waiting for transfers between devices, local(): lax.all_gather(key_rot, 'sp', axis=0, tiled=True)  14.3 us
  transfers between devices with their start and end apart: 7, of which 6 were waited for; matrix products, arithmetic and copies ran while one was open for 22% of the time, Pallas kernels for 0%

commit v1 on v0

--- a/solution.py
+++ b/solution.py
@@ -108,7 +108,12 @@
         middle * lax.rsqrt(jnp.mean(middle * middle, axis=-1, keepdims=True) + 1e-06) * norm_gain
     )
     normed = normed.astype(jnp.bfloat16)
-    rows_all = lax.all_gather(normed, "tp", axis=0, tiled=True)
+    ring = [normed]
+    for hop in range(3):
+        ring.append(lax.ppermute(ring[-1], "tp", [(dev, (dev + 1) % 4) for dev in range(4)]))
+    rows_all = jnp.roll(
+        jnp.concatenate(ring[::-1], axis=0), (lax.axis_index("tp") + 1) * ring[0].shape[0], axis=0
+    )
     pieces = (
         lax.all_gather(gate_weight, "sp", axis=0, tiled=True),
         lax.all_gather(up_weight, "sp", axis=0, tiled=True),

time: 362 us -> 316 us (0.87)
  waiting for transfers between devices: 230 us -> 169 us
  local copies, waits for them, and re-layouts: 15.3 us -> 29.2 us
    all_gather x1, waiting for transfers between devices: 52.7 us -> 0.01 us  [local(): lax.all_gather(up_weight, 'sp', axis=0, tiled=True)]
    ppermute x0 -> x3, waiting for transfers between devices: none -> 43.3 us  [local(): lax.ppermute(ring[-1], 'tp', [(dev, (dev + 1) % 4) for dev in range(4)])]
    all_gather x1 -> x0, waiting for transfers between devices: 31.5 us -> none  [local(): rows_all = lax.all_gather(normed, 'tp', axis=0, tiled=True)]
    all_gather x1, waiting for transfers between devices: 59.3 us -> 40 us  [local(): down_all = lax.all_gather(down_weight, 'sp', axis=1, tiled=True)]
    unnamed x10 -> x18, local copies, waits for them, and re-layouts: 2.17 us -> 16.1 us
  transfers between devices with their start and end apart: 7 -> 9, of which waited for: 6 -> 7; matrix products, arithmetic and copies ran while one was open for 22% -> 31% of each run, Pallas kernels for 0% -> 0%
where the time goes in v1:
time: 316 us
  waiting for transfers between devices  169 us (53%)
  matrix products  53.7 us (17%)
  other arithmetic  38.1 us (12%)
  local copies, waits for them, and re-layouts  29.2 us (9%)
  between operations  13.8 us (4%)
  blocking collectives  11.2 us (4%)
    reduce_scatter x1, waiting for transfers between devices, local(): lax.psum_scatter(jnp.dot(hidden, down_all, preferred_element_type=jnp.flo...  43.4 us
    ppermute x3, waiting for transfers between devices, local(): lax.ppermute(ring[-1], 'tp', [(dev, (dev + 1) % 4) for dev in range(4)])  43.3 us
    all_gather x1, waiting for transfers between devices, local(): down_all = lax.all_gather(down_weight, 'sp', axis=1, tiled=True)  40 us
    all_gather x1, waiting for transfers between devices, local(): lax.all_gather(value_block, 'sp', axis=0, tiled=True)  27.3 us
    reduce_sum x4, other arithmetic, attend_block(): denominator = denominator * factor + jnp.sum(raised, axis=1)  20 us
    dot_general x4, matrix products, attend_block(): lax.dot_general(query_rot, key_part, (((1,), (1,)), ((), ())), preferred_...  18 us
    unnamed x18, local copies, waits for them, and re-layouts  16.1 us
    all_gather x1, waiting for transfers between devices, local(): lax.all_gather(key_rot, 'sp', axis=0, tiled=True)  13.8 us
  transfers between devices with their start and end apart: 9, of which 7 were waited for; matrix products, arithmetic and copies ran while one was open for 31% of the time, Pallas kernels for 0%

profile of v1, /device:TPU:0, one launch (start us, length us, event | category | flops | bytes accessed | tf_op | source)
XLA Modules:
  0.0 315.6 jit_solution(2938891268032677530)
XLA Ops:
  6.6 1.2 fusion.27
  7.8 1.2 fusion.28
  9.2 0.3 reshape.338
  9.5 0.4 fusion.46
  10.1 1.0 subtract_convert_fusion.1
  11.1 0.3 copy.34
  11.4 0.8 convert_element_type.62
  12.3 0.7 constant_dynamic-slice_fusion
  13.1 0.7 all-gather.12.cloned.1.call-update
  13.9 0.5 all-gather.10.cloned.1.call-update
  14.4 1.0 convert_multiply_fusion.2
  15.5 0.2 copy.35
  15.7 2.7 mul.251
  18.5 2.4 reduce_sum.37
  21.1 1.6 reshape.340
  22.8 1.1 fusion.30
  24.0 1.7 multiply_multiply_fusion
  25.6 1.4 subtract_convert_fusion
  27.1 1.2 pad_maximum_fusion
  28.3 0.5 copy.37
  28.8 0.5 copy.43
  29.4 13.8 %all-gather.6.cloned.1.call-done = bf16[4096,128]{0,1:T(8,128)(2,1)} async-done(((bf16[1024,128]{0,1:T(8,128)(2,1)}), bf16[4096,128]{0,1:T(8,128)(2,1)}) %all-gather.6.cloned.1.call-update) | async-done | bytes 1048592 | tf_op jit(solution)/shard_map/all_gather | solution.py:88
  43.1 1.6 copy.42
  44.7 27.3 %all-gather.8.cloned.1.call-done = bf16[4096,128]{1,0:T(8,128)(2,1)} async-done(((bf16[1024,128]{1,0:T(8,128)(2,1)}), bf16[4096,128]{1,0:T(8,128)(2,1)}) %all-gather.8.cloned.1.call-update) | async-done | bytes 1048592 | tf_op jit(solution)/shard_map/all_gather | solution.py:89
  72.1 53.6 %while.15 = (s32[]{:T(128)}, f32[2048]{0:T(1024)S(1)}, f32[2048]{0:T(1024)S(1)}, f32[2048,128]{1,0:T(8,128)S(1)}, bf16[4,1024,128]{2,1,0:T(8,128)(2,1)S(1)}, /*i...) while((s32[]{:T(128)}, f32[2048]{0:T(1024)S(1)}, ...), condition=%wide.region_5.6_spmd.clone, body=%wide.region_2.5_spmd.clone.sunk | while | flops 1091315712 | bytes 61997704 | solution.py:96
  72.1 4.5 %multiply_reduce_fusion.3 = (f32[2048]{0:T(1024)S(1)}, f32[1024,2048]{1,0:T(8,128)}) fusion(bf16[2048,128]{1,0:T(8,128)(2,1)S(1)} %get-tuple-element.200, bf16[4,1024,128]{2,1,0:T(8,128)(2,1)S(1)} %get-tuple-element.199, s32[]{:T(128)} %get-tuple-element.186), kind=kOutput, calls=%fused_computation.1.clone.1 | convolution fusion | flops 541063168 | bytes 9183236 | tf_op jit(solution)/shard_map/while/body/eval_jaxpr/dot_general | solution.py:67
  76.6 5.1 %fusion.62 = f32[2048]{0:T(1024)S(1)} fusion(f32[1024,2048]{1,0:T(8,128)} %get-tuple-element.174, f32[2048]{0:T(1024)S(1)} %select_maximum_fusion.2), kind=kLoop, calls=%fused_computation.3.clone.1 | loop fusion | flops 6289408 | bytes 8404992 | tf_op jit(solution)/shard_map/while/body/eval_jaxpr/reduce_sum | solution.py:75
  81.7 1.3 copy-done.2
  83.0 2.9 fusion.64
  86.0 4.5 %multiply_reduce_fusion.3 = (f32[2048]{0:T(1024)S(1)}, f32[1024,2048]{1,0:T(8,128)}) fusion(bf16[2048,128]{1,0:T(8,128)(2,1)S(1)} %get-tuple-element.200, bf16[4,1024,128]{2,1,0:T(8,128)(2,1)S(1)} %get-tuple-element.199, s32[]{:T(128)} %get-tuple-element.186), kind=kOutput, calls=%fused_computation.1.clone.1 | convolution fusion | flops 541063168 | bytes 9183236 | tf_op jit(solution)/shard_map/while/body/eval_jaxpr/dot_general | solution.py:67
  90.5 5.0 %fusion.62 = f32[2048]{0:T(1024)S(1)} fusion(f32[1024,2048]{1,0:T(8,128)} %get-tuple-element.174, f32[2048]{0:T(1024)S(1)} %select_maximum_fusion.2), kind=kLoop, calls=%fused_computation.3.clone.1 | loop fusion | flops 6289408 | bytes 8404992 | tf_op jit(solution)/shard_map/while/body/eval_jaxpr/reduce_sum | solution.py:75
  95.4 0.9 copy-done.2
  96.3 2.9 fusion.64
  99.2 4.5 %multiply_reduce_fusion.3 = (f32[2048]{0:T(1024)S(1)}, f32[1024,2048]{1,0:T(8,128)}) fusion(bf16[2048,128]{1,0:T(8,128)(2,1)S(1)} %get-tuple-element.200, bf16[4,1024,128]{2,1,0:T(8,128)(2,1)S(1)} %get-tuple-element.199, s32[]{:T(128)} %get-tuple-element.186), kind=kOutput, calls=%fused_computation.1.clone.1 | convolution fusion | flops 541063168 | bytes 9183236 | tf_op jit(solution)/shard_map/while/body/eval_jaxpr/dot_general | solution.py:67
  103.7 5.0 %fusion.62 = f32[2048]{0:T(1024)S(1)} fusion(f32[1024,2048]{1,0:T(8,128)} %get-tuple-element.174, f32[2048]{0:T(1024)S(1)} %select_maximum_fusion.2), kind=kLoop, calls=%fused_computation.3.clone.1 | loop fusion | flops 6289408 | bytes 8404992 | tf_op jit(solution)/shard_map/while/body/eval_jaxpr/reduce_sum | solution.py:75
  108.7 0.8 copy-done.2
  109.6 2.9 fusion.64
  112.5 4.5 %multiply_reduce_fusion.3 = (f32[2048]{0:T(1024)S(1)}, f32[1024,2048]{1,0:T(8,128)}) fusion(bf16[2048,128]{1,0:T(8,128)(2,1)S(1)} %get-tuple-element.200, bf16[4,1024,128]{2,1,0:T(8,128)(2,1)S(1)} %get-tuple-element.199, s32[]{:T(128)} %get-tuple-element.186), kind=kOutput, calls=%fused_computation.1.clone.1 | convolution fusion | flops 541063168 | bytes 9183236 | tf_op jit(solution)/shard_map/while/body/eval_jaxpr/dot_general | solution.py:67
  117.0 5.0 %fusion.62 = f32[2048]{0:T(1024)S(1)} fusion(f32[1024,2048]{1,0:T(8,128)} %get-tuple-element.174, f32[2048]{0:T(1024)S(1)} %select_maximum_fusion.2), kind=kLoop, calls=%fused_computation.3.clone.1 | loop fusion | flops 6289408 | bytes 8404992 | tf_op jit(solution)/shard_map/while/body/eval_jaxpr/reduce_sum | solution.py:75
  122.0 0.8 copy-done.2
  122.8 2.9 fusion.64
  125.7 0.3 divide_convert_fusion
  126.0 0.5 copy.51
  126.6 0.3 all_to_all.14
  126.9 11.2 %all_to_all.19 = bf16[4,256,256]{2,1,0:T(8,128)(2,1)S(1)} all-to-all(bf16[4,256,256]{2,1,0:T(8,128)(2,1)S(1)} %all_to_all.14), channel_id=1, replica_groups=mesh['grp'=2,'sp'=4,'tp'=4] {'tp'}, dimensions={0} | all-to-all | bytes 1048576 | tf_op jit(solution)/shard_map/all_to_all | solution.py:104
  138.2 0.2 copy.41
  138.4 4.2 %multiply_reduce_fusion.1 = (f32[256]{0:T(256)S(1)}, f32[256,2048]{1,0:T(8,128)S(1)}) fusion(bf16[256,1024]{0,1:T(8,128)(2,1)S(1)} %bitcast.44, bf16[1024,2048]{1,0:T(8,128)(2,1)} %param.18, bf16[256,2048]{1,0:T(8,128)(2,1)} %param.19), kind=kOutput, calls=%fused_computation.30 | convolution fusion | flops 1075838720 | bytes 7865344 | tf_op jit(solution)/shard_map/dot_general | solution.py:105
  142.6 0.2 multiply_convert_fusion.1
  142.9 14.3 %collective-permute-done = bf16[256,2048]{1,0:T(8,128)(2,1)} collective-permute-done((bf16[256,2048]{1,0:T(8,128)(2,1)S(1)}, bf16[256,2048]{1,0:T(8,128)(2,1)}, u32[]{:S(2)}, u32[]{:S(2)}) %collective-permute-start) | collective-permute-done | bytes 1048608 | tf_op jit(solution)/shard_map/ppermute | solution.py:113
  157.3 14.5 %collective-permute-done.1 = bf16[256,2048]{1,0:T(8,128)(2,1)} collective-permute-done((bf16[256,2048]{1,0:T(8,128)(2,1)}, bf16[256,2048]{1,0:T(8,128)(2,1)}, u32[]{:S(2)}, u32[]{:S(2)}) %collective-permute-start.1) | collective-permute-done | bytes 1048608 | tf_op jit(solution)/shard_map/ppermute | solution.py:113
  171.8 14.5 %collective-permute-done.2 = bf16[256,2048]{1,0:T(8,128)(2,1)} collective-permute-done((bf16[256,2048]{1,0:T(8,128)(2,1)}, bf16[256,2048]{1,0:T(8,128)(2,1)}, u32[]{:S(2)}, u32[]{:S(2)}) %collective-permute-start.2) | collective-permute-done | bytes 1048608 | tf_op jit(solution)/shard_map/ppermute | solution.py:113
  186.3 2.3 constant_dynamic-update-slice_fusion.7
  188.7 2.3 constant_dynamic-update-slice_fusion.6
  191.0 2.3 constant_dynamic-update-slice_fusion.5
  193.3 1.2 constant_dynamic-update-slice_fusion.4
  194.5 2.3 constant_dynamic-update-slice_fusion.3
  196.8 2.4 constant_dynamic-update-slice_fusion.2
  199.2 2.4 constant_dynamic-update-slice_fusion.1
  201.5 1.3 constant_dynamic-update-slice_fusion
  202.8 7.8 %fusion.18 = f32[1024,704]{0,1:T(8,128)} fusion(bf16[2048,704]{0,1:T(8,128)(2,1)} %all-gather.12.cloned.1.call-done, bf16[2048,2048]{1,0:T(8,128)(2,1)} %constant_dynamic-update-slice_fusion, s32[]{:T(128)S(6)} %select_n.48), kind=kOutput, calls=%fused_computation.22 | convolution fusion | flops 2952790016 | bytes 9961476 | tf_op jit(solution)/shard_map/dot_general | solution.py:122
  210.7 40.0 %all-gather.14.cloned.1.call-done = bf16[704,2048]{1,0:T(8,128)(2,1)} async-done(((bf16[704,512]{1,0:T(8,128)(2,1)}), bf16[704,2048]{1,0:T(8,128)(2,1)}) %all-gather.14.cloned.1.call-update) | async-done | bytes 2883600 | tf_op jit(solution)/shard_map/all_gather | solution.py:123
  250.7 12.1 %convolution_convert_fusion = bf16[1024,2048]{1,0:T(8,128)(2,1)} fusion(bf16[704,2048]{1,0:T(8,128)(2,1)} %all-gather.14.cloned.1.call-done, f32[1024,704]{0,1:T(8,128)} %fusion.18, bf16[2048,704]{0,1:T(8,128)(2,1)} %all-gather.10.cloned.1.call-done, bf16[2048,2048]{1,0:T(8,128)(2,1)} %constant_dynamic-update-slice_fusion, s32[]{:T(128)S(6)} %select_n.48), kind=kOutput, calls=%fused_computation.21 | convolution fusion | flops 5912002560 | bytes 17039364 | tf_op jit(solution)/shard_map/dot_general | solution.py:126
  262.8 43.4 %reduce-scatter.2.cloned.1.call-done = bf16[256,2048]{1,0:T(8,128)(2,1)} async-done(((bf16[1024,2048]{1,0:T(8,128)(2,1)}), bf16[256,2048]{1,0:T(8,128)(2,1)}) %reduce-scatter.2.cloned.1.call-update) | async-done | bytes 1048592 | tf_op jit(solution)/shard_map/reduce_scatter | solution.py:125
  306.2 2.5 add_convert_fusion
  (54 shorter events, 1.1 us)
Async XLA Ops:
  6.5 5.8 %copy-start = (bf16[1024,256]{1,0:T(8,128)(2,1)S(1)}, bf16[1024,256]{1,0:T(8,128)(2,1)}, u32[]{:S(2)}) copy-start(bf16[1024,256]{1,0:T(8,128)(2,1)} %param.15) | copy-start | bytes 1572868
  6.5 36.6 %all-gather.6.cloned.1.call-start = ((), (), s32[]{:S(2)}) async-start(), calls=%async_computation.2 | async-start | bytes 1310720 | tf_op jit(solution)/shard_map/all_gather | solution.py:88
  9.0 5.5 %copy-start.3 = (bf16[1024,256]{1,0:T(8,128)(2,1)S(1)}, bf16[1024,256]{1,0:T(8,128)(2,1)}, u32[]{:S(2)}) copy-start(bf16[1024,256]{1,0:T(8,128)(2,1)} %param.13) | copy-start | bytes 1572868
  12.3 59.8 %all-gather.8.cloned.1.call-start = ((), (), s32[]{:S(2)}) async-start(), calls=%async_computation.3 | async-start | bytes 1310720 | tf_op jit(solution)/shard_map/all_gather | solution.py:89
  13.1 189.8 %all-gather.12.cloned.1.call-start = ((), (), s32[]{:S(2)}) async-start(), calls=%async_computation.5 | async-start | bytes 3604480 | tf_op jit(solution)/shard_map/all_gather | solution.py:119
  13.8 196.8 %all-gather.10.cloned.1.call-start = ((), (), s32[]{:S(2)}) async-start(), calls=%async_computation.4 | async-start | bytes 3604480 | tf_op jit(solution)/shard_map/all_gather | solution.py:118
  14.4 236.3 %all-gather.14.cloned.1.call-start = ((), (), s32[]{:S(2)}) async-start(), calls=%async_computation.6 | async-start | bytes 3604480 | tf_op jit(solution)/shard_map/all_gather | solution.py:123
  15.5 7.2 %copy-start.5 = (f32[128]{0:T(128)S(1)}, f32[128]{0:T(128)}, u32[]{:S(2)}) copy-start(f32[128]{0:T(128)} %param.16) | copy-start | bytes 1540
  76.6 6.5 %copy-start.2 = (f32[1024,2048]{1,0:T(8,128)S(1)}, f32[1024,2048]{1,0:T(8,128)}, u32[]{:S(2)}) copy-start(f32[1024,2048]{1,0:T(8,128)} %get-tuple-element.174) | copy-start | bytes 25165828 | tf_op jit(solution)/shard_map/while
  90.5 5.9 %copy-start.2 = (f32[1024,2048]{1,0:T(8,128)S(1)}, f32[1024,2048]{1,0:T(8,128)}, u32[]{:S(2)}) copy-start(f32[1024,2048]{1,0:T(8,128)} %get-tuple-element.174) | copy-start | bytes 25165828 | tf_op jit(solution)/shard_map/while
  103.7 5.8 %copy-start.2 = (f32[1024,2048]{1,0:T(8,128)S(1)}, f32[1024,2048]{1,0:T(8,128)}, u32[]{:S(2)}) copy-start(f32[1024,2048]{1,0:T(8,128)} %get-tuple-element.174) | copy-start | bytes 25165828 | tf_op jit(solution)/shard_map/while
  117.0 5.8 %copy-start.2 = (f32[1024,2048]{1,0:T(8,128)S(1)}, f32[1024,2048]{1,0:T(8,128)}, u32[]{:S(2)}) copy-start(f32[1024,2048]{1,0:T(8,128)} %get-tuple-element.174) | copy-start | bytes 25165828 | tf_op jit(solution)/shard_map/while
  138.4 4.3 %copy-start.4 = (f32[2048]{0:T(1024)S(1)}, f32[2048]{0:T(1024)}, u32[]{:S(2)}) copy-start(f32[2048]{0:T(1024)} %param.20) | copy-start | bytes 24580
  142.9 14.4 %collective-permute-start = (bf16[256,2048]{1,0:T(8,128)(2,1)S(1)}, bf16[256,2048]{1,0:T(8,128)(2,1)}, u32[]{:S(2)}, u32[]{:S(2)}) collective-permute-start(bf16[256,2048]{1,0:T(8,128)(2,1)S(1)} %multiply_convert_fusion.1), channel_id=1, source_target_pairs={{0,1},{1,2},{2,3},{3,0},{4,5},{5,6},{6,7},{7,4},{8,9},{9,10},{10,1... | collective-permute-start | bytes 3145736 | tf_op jit(solution)/shard_map/ppermute | solution.py:113
  157.3 14.5 %collective-permute-start.1 = (bf16[256,2048]{1,0:T(8,128)(2,1)}, bf16[256,2048]{1,0:T(8,128)(2,1)}, u32[]{:S(2)}, u32[]{:S(2)}) collective-permute-start(bf16[256,2048]{1,0:T(8,128)(2,1)} %collective-permute-done), channel_id=1, source_target_pairs={{0,1},{1,2},{2,3},{3,0},{4,5},{5,6},{6,7},{7,4},{8,9},{9,10},{10,1... | collective-permute-start | bytes 3145736 | tf_op jit(solution)/shard_map/ppermute | solution.py:113
  157.3 149.0 %reduce-scatter.2.cloned.1.call-start = ((), (), s32[]{:S(2)}) async-start(), calls=%async_computation.7 | async-start | bytes 5242880 | tf_op jit(solution)/shard_map/reduce_scatter | solution.py:125
  171.8 14.5 %collective-permute-start.2 = (bf16[256,2048]{1,0:T(8,128)(2,1)}, bf16[256,2048]{1,0:T(8,128)(2,1)}, u32[]{:S(2)}, u32[]{:S(2)}) collective-permute-start(bf16[256,2048]{1,0:T(8,128)(2,1)} %collective-permute-done.1), channel_id=1, source_target_pairs={{0,1},{1,2},{2,3},{3,0},{4,5},{5,6},{6,7},{7,4},{8,9},{9,10},{10,1... | collective-permute-start | bytes 3145736 | tf_op jit(solution)/shard_map/ppermute | solution.py:113
  262.8 45.9 %copy-start.1 = (bf16[1024,256]{1,0:T(8,128)(2,1)S(1)}, bf16[1024,256]{1,0:T(8,128)(2,1)}, u32[]{:S(2)}) copy-start(bf16[1024,256]{1,0:T(8,128)(2,1)} %param.15) | copy-start | bytes 1572868
Sparse Core Ops, SparseCore 0:
  12.4 30.6 all-gather.5
  44.7 27.3 all-gather.7
  73.7 58.4 all-gather.11
  133.6 57.7 all-gather.9
  192.9 57.7 all-gather.13
  263.0 43.2 reduce-scatter.1
